TPU v7x, 512 devices: a whole 4x8x8 slice. The times are simulated.
512 devices in a mesh: sp: 32 (over z, x), tp: 16 (over y, core).
Axes of the slice: x: 4, y: 8, z: 8, core: 2. Of those that a mesh axis runs over, the one named last changes fastest.
Arguments:
- pool_input: bfloat16 [1024, 12288], P('tp', 'sp'), may hold values from -6 to 6
- pool_gate: bfloat16 [1024, 12288], P('tp', 'sp'), may hold values from -6 to 6
- pool_mix: bfloat16 [4, 256, 256], replicated, may hold values from -0.375 to 0.375
- pool_scale: float32 [1024], replicated, may hold values from 0.1 to 1.9
- out_proj: bfloat16 [1024, 2048], P(None, 'tp'), may hold values from -0.375 to 0.375
- residual: bfloat16 [12288, 2048], P('sp', 'tp'), may hold values from -12 to 12
- norm_gain: float32 [2048], P('tp'), may hold values from 0.1 to 1.9
- routes: int32 [12288, 2], P('sp'), may hold values from 0 to 31, all different within a row; in each aligned block of 384 rows (0 to 383, 384 to 767, ...) at most 36 rows name the same one
- group_logits: float32 [12288, 4], P('sp'), may hold values from -4 to 4
- expert_scores: float32 [12288, 2], P('sp'), may hold values from -4 to 4
- w_gate: bfloat16 [32, 2048, 4096], P('sp', None, 'tp'), may hold values from -0.125 to 0.125
- w_up: bfloat16 [32, 2048, 4096], P('sp', None, 'tp'), may hold values from -0.125 to 0.125
- w_down: bfloat16 [32, 4096, 2048], P('sp', None, 'tp'), may hold values from -0.375 to 0.375
Outputs:
- layer_out: bfloat16 [12288, 2048], P('sp', 'tp')
Inputs may be any that keep to these rules, and one draw needn't show every extreme that they name: `routes`: among the rows of one device (aligned blocks of 384 rows) no expert is named by more than 36 rows, a bound that some block reaches; the 2 experts of a row differ.
All inputs are finite; a program needn't handle non-finite values.
Results may differ from a plain program's by a relative error of at most 0.01.
Values may be sent and summed in bfloat16 or wider, within the bound.
No kernel may reach another device: no remote copies, remote signals or barrier semaphores. Data moves between devices by JAX's collectives and lax.ppermute only.
A program may use at most 64 MiB of HBM per device.

v0:
```python
import jax
import jax.numpy as jnp
from jax import lax
from jax.sharding import PartitionSpec as P

D = 2048
POOL_GROUP = 256
TOP = 2
reach_back = 15
epsilon = 1e-06


def from_behind(value, axis, steps):
    count = lax.axis_size(axis)
    initial, last = (max(0, -steps), min(count, count - steps))
    return lax.ppermute(value, axis, [(source, source + steps) for source in range(initial, last)])


def in_one_piece(arrays, axis, dim, along):
    ends, at = ([], 0)
    for a in arrays[:-1]:
        at += a.shape[along]
        ends.append(at)
    both = jnp.concatenate(arrays, axis=along)
    return tuple(jnp.split(lax.all_gather(both, axis, axis=dim, tiled=True), ends, axis=along))


def from_everyone(value, axis):
    count = lax.axis_size(axis)
    return lax.all_to_all(
        jnp.broadcast_to(value[None], (count, *value.shape)), axis, 0, 0, tiled=True
    )


def over_copies(value, axis):
    return from_everyone(value, axis).sum(axis=0)


def window_terms(extended, first_channel, first_position, group_width):
    length = extended.shape[1] - reach_back
    layered = extended
    stride = 1
    partial_sums = []
    for _ in range(4):
        layered = layered[:, stride:] + layered[:, :-stride]
        stride = stride * 2
        partial_sums.append(layered[:, layered.shape[1] - length :])
    channel = first_channel + jnp.arange(extended.shape[0], dtype=jnp.int32)
    scale_index = channel // group_width
    chosen = partial_sums[3]
    for octave in range(3):
        chosen = jnp.where((scale_index == octave)[:, None], partial_sums[octave], chosen)
    window = (2 ** (scale_index + 1)).astype(jnp.float32)
    positions = (first_position + jnp.arange(length, dtype=jnp.int32) + 1).astype(jnp.float32)
    counted = jnp.minimum(positions[None, :], window[:, None])
    return chosen / counted - extended[:, reach_back:]


def slot_table(row_block, experts, capacity):
    flattened = row_block.reshape(-1)
    onehot = (flattened[:, None] == jnp.arange(experts, dtype=jnp.int32)[None, :]).astype(jnp.int32)
    before = jnp.cumsum(onehot, axis=0) - onehot
    ranked = jnp.sum(before * onehot, axis=1)
    return flattened * capacity + ranked


def route_weights(routes, group_logits, expert_scores, per_group):
    raised = jnp.exp(group_logits)
    group_prob = raised / jnp.sum(raised, axis=1, keepdims=True)
    owning_group = routes // per_group
    groups_iota = jnp.arange(group_logits.shape[1], dtype=jnp.int32)
    picked = jnp.sum(
        jnp.where(
            owning_group[:, :, None] == groups_iota[None, None, :], group_prob[:, None, :], 0.0
        ),
        axis=2,
    )
    lifted = jnp.exp(expert_scores)
    return picked * lifted / jnp.sum(lifted, axis=1, keepdims=True)


def per_device(
    pool_input,
    pool_gate,
    pool_mix,
    pool_scale,
    out_proj,
    residual,
    norm_gain,
    routes,
    group_logits,
    expert_scores,
    w_gate,
    w_up,
    w_down,
):
    channels, length = pool_input.shape
    edge_rows = from_behind(pool_input[:, length - reach_back :], "sp", 1)
    extended = jnp.concatenate([edge_rows, pool_input], axis=1).astype(jnp.float32)
    first_channel = lax.axis_index("tp") * channels
    first_position = lax.axis_index("sp") * length
    pooled = window_terms(extended, first_channel, first_position, POOL_GROUP).astype(jnp.bfloat16)
    gathered, gate_rows = in_one_piece((pooled, pool_gate), "tp", 0, 1)
    scales = pool_mix.shape[0]
    mixed_rows = jnp.einsum(
        "gct,gcd->tgd",
        gathered.reshape(scales, POOL_GROUP, length),
        pool_mix,
        preferred_element_type=jnp.float32,
    ).reshape(length, scales * POOL_GROUP)
    branch = (
        jax.nn.sigmoid(gate_rows.T.astype(jnp.float32)) * mixed_rows * pool_scale[None, :]
    ).astype(jnp.bfloat16)
    hidden_state = (
        residual.astype(jnp.float32) + jnp.dot(branch, out_proj, preferred_element_type=jnp.float32)
    ).astype(jnp.bfloat16)
    state_float = hidden_state.astype(jnp.float32)
    squares = over_copies(jnp.sum(state_float * state_float, axis=1), "tp")
    normed = (state_float * lax.rsqrt(squares / D + epsilon)[:, None] * norm_gain[None, :]).astype(
        jnp.bfloat16
    )
    experts = lax.axis_size("sp") * w_gate.shape[0]
    weights = route_weights(routes, group_logits, expert_scores, experts // group_logits.shape[1])
    capacity = 3 * TOP * length // (2 * experts)
    destination = slot_table(routes, experts, capacity)
    token_index = jnp.arange(length * TOP, dtype=jnp.int32) // TOP
    sources = jnp.full((experts * capacity,), length, jnp.int32).at[destination].set(token_index)
    padded = jnp.concatenate([normed, jnp.zeros((1, normed.shape[1]), jnp.bfloat16)], axis=0)
    arrived = lax.all_to_all(padded[sources], "sp", split_axis=0, concat_axis=0, tiled=True)
    portion = lax.all_gather(arrived, "tp", axis=1, tiled=True)
    rows_gate = w_gate[0]
    rows_up = w_up[0]
    gate_term = jnp.dot(portion, rows_gate, preferred_element_type=jnp.float32)
    up_term = jnp.dot(portion, rows_up, preferred_element_type=jnp.float32)
    activated = (jax.nn.silu(gate_term) * up_term).astype(jnp.bfloat16)
    rows_down = w_down[0]
    result = jnp.dot(
        lax.all_gather(activated, "tp", axis=1, tiled=True),
        rows_down,
        preferred_element_type=jnp.float32,
    ).astype(jnp.bfloat16)
    returned = lax.all_to_all(result, "sp", split_axis=0, concat_axis=0, tiled=True)
    picked = returned[destination].astype(jnp.float32).reshape(length, TOP, returned.shape[1])
    combined = jnp.sum(weights[:, :, None] * picked, axis=1)
    return (state_float + combined).astype(jnp.bfloat16)


def solution(mesh):
    placed = (
        P("tp", "sp"),
        P("tp", "sp"),
        P(),
        P(),
        P(None, "tp"),
        P("sp", "tp"),
        P("tp"),
        P("sp", None),
        P("sp", None),
        P("sp", None),
        P("sp", None, "tp"),
        P("sp", None, "tp"),
        P("sp", None, "tp"),
    )
    return jax.shard_map(
        per_device, mesh=mesh, in_specs=placed, out_specs=P("sp", "tp"), check_vma=False
    )
```

profile of v0, /device:TPU:16, one launch (start us, length us, event | category | flops | bytes accessed | tf_op | source)
XLA Modules:
  0.0 268.7 jit_solution(10977367310961019468)
XLA Ops:
  6.5 0.9 slice.43
  7.4 3.4 %collective-permute-start = (bf16[64,15]{1,0:T(8,128)(2,1)S(1)}, bf16[64,15]{1,0:T(8,128)(2,1)S(1)}, u32[]{:S(2)}, u32[]{:S(2)}) collective-permute-start(bf16[64,15]{1,0:T(8,128)(2,1)S(1)} %slice.43), channel_id=1, source_target_pairs={{0,16},{16,32},{32,48},{48,64},{64,80},{80,96},{96,112},{112,128},... | collective-permute-start | bytes 5768 | tf_op jit(solution)/shard_map/ppermute | solution.py:16
  10.9 1.3 collective-permute-done
  12.2 0.9 maximum_convert_fusion
  13.1 0.1 slice_add_fusion.2
  13.2 0.1 slice_add_fusion.1
  13.3 0.1 slice_add_fusion
  13.5 0.2 fusion.13
  13.7 0.7 pad_maximum_fusion
  14.4 0.1 copy.36
  14.5 0.1 eq.69
  14.7 0.1 eq.65
  14.8 1.7 reduce-window.6
  16.6 0.3 slice_reduce_fusion
  16.9 0.1 copy.35
  17.0 0.2 mul.134
  17.2 0.1 fusion.12
  17.3 3.4 %scatter_custom_fusion = s32[1152]{0:T(1024)S(1)} fusion(s32[768]{0:T(1024)S(1)} %fusion.24, s32[768]{0:T(1024)S(1)} %add_select_fusion, s32[]{:T(128)} %constant.90.clone.1), kind=kCustom, calls=%fused_computation.60 | custom fusion | bytes 4612 | tf_op jit(solution)/shard_map/scatter | solution.py:127
  20.7 39.9 %all-gather.4.cloned.1.call-done = bf16[1024,768]{1,0:T(8,128)(2,1)} async-done(((bf16[64,768]{1,0:T(8,128)(2,1)}), bf16[1024,768]{1,0:T(8,128)(2,1)}) %all-gather.4.cloned.1.call-update) | async-done | bytes 1572880 | tf_op jit(solution)/shard_map/all_gather | solution.py:25
  60.7 1.6 slice-done
  62.3 0.5 fusion.26
  62.8 0.4 fusion.2
  63.3 0.5 copy-done.3
  63.7 0.0 copy-done.4
  63.8 0.5 multiply_reduce_fusion
  64.3 0.6 broadcast_in_dim.69
  64.9 6.4 %all-to-all-start = ((f32[16,1,384]{2,1,0:T(1,128)}), f32[16,1,384]{2,1,0:T(1,128)S(1)}, u32[]{:S(2)}, u32[]{:S(2)}) async-start(f32[16,1,384]{2,1,0:T(1,128)} %broadcast_in_dim.69), calls=%async_computation | async-start | bytes 49152 | tf_op jit(solution)/shard_map/all_to_all | solution.py:30
  71.3 0.0 all-gather.6.cloned.1.call-start
  71.3 5.4 %all-to-all-done = f32[16,1,384]{2,1,0:T(1,128)S(1)} async-done(((f32[16,1,384]{2,1,0:T(1,128)}), f32[16,1,384]{2,1,0:T(1,128)S(1)}, u32[]{:S(2)}, u32[]{:S(2)}) %all-to-all-start) | async-done | bytes 24608 | tf_op jit(solution)/shard_map/all_to_all | solution.py:30
  76.8 0.1 multiply_convert_fusion
  76.9 2.9 %gather_fusion = bf16[1152,128]{1,0:T(8,128)(2,1)S(1)} fusion(bf16[385,128]{1,0:T(8,128)(2,1)S(1)} %concatenate.11, s32[2048]{0:T(1024)S(1)} %pad_clamp_fusion), kind=kCustom, calls=%fused_computation | custom fusion | bytes 594432 | tf_op jit(solution)/shard_map/gather | solution.py:129
  79.8 0.1 all_to_all.21
  79.9 24.5 %all_to_all.30 = bf16[32,36,128]{2,1,0:T(8,128)(2,1)S(1)} all-to-all(bf16[32,36,128]{2,1,0:T(8,128)(2,1)S(1)} %all_to_all.21), channel_id=1, replica_groups=mesh['sp'=32,'tp'=16] {'sp'}, dimensions={0} | all-to-all | bytes 589824 | tf_op jit(solution)/shard_map/all_to_all | solution.py:129
  104.4 0.8 all_to_all.23
  105.2 0.0 all-gather.8.cloned.1.call-start
  105.2 45.1 %all-gather.6.cloned.1.call-done = bf16[1152,2048]{1,0:T(8,128)(2,1)} async-done(((bf16[1152,128]{1,0:T(8,128)(2,1)}), bf16[1152,2048]{1,0:T(8,128)(2,1)}) %all-gather.6.cloned.1.call-update) | async-done | bytes 4718608 | tf_op jit(solution)/shard_map/all_gather | solution.py:130
  150.3 3.9 %fusion.7 = f32[1152,256]{1,0:T(8,128)S(1)} fusion(bf16[1152,2048]{1,0:T(8,128)(2,1)} %all-gather.6.cloned.1.call-done, bf16[1,2048,256]{2,1,0:T(8,128)(2,1)S(1)} %copy-done), kind=kOutput, calls=%fused_computation.14 | convolution fusion | flops 1207959552 | bytes 6946816 | tf_op jit(solution)/shard_map/dot_general | solution.py:133
  154.2 2.3 fusion
  156.7 71.4 %all-gather.8.cloned.1.call-done = bf16[1152,4096]{1,0:T(8,128)(2,1)} async-done(((bf16[1152,256]{1,0:T(8,128)(2,1)}), bf16[1152,4096]{1,0:T(8,128)(2,1)}) %all-gather.8.cloned.1.call-update) | async-done | bytes 9437200 | tf_op jit(solution)/shard_map/all_gather | solution.py:138
  228.1 6.5 %convolution_convert_fusion = bf16[1152,128]{1,0:T(8,128)(2,1)S(1)} fusion(bf16[1152,4096]{1,0:T(8,128)(2,1)} %all-gather.8.cloned.1.call-done, bf16[1,4096,128]{2,1,0:T(8,128)(2,1)} %param.25), kind=kOutput, calls=%fused_computation.5 | convolution fusion | flops 1208107008 | bytes 10780672 | tf_op jit(solution)/shard_map/dot_general | solution.py:137
  234.6 0.8 all_to_all.24
  235.3 9.0 %all-to-all-start.2 = ((bf16[32,36,128]{2,1,0:T(8,128)(2,1)}), bf16[32,36,128]{2,1,0:T(8,128)(2,1)S(1)}, u32[]{:S(2)}, u32[]{:S(2)}) async-start(bf16[32,36,128]{2,1,0:T(8,128)(2,1)} %all_to_all.24), calls=%async_computation.2 | async-start | bytes 655360 | tf_op jit(solution)/shard_map/all_to_all | solution.py:142
  244.4 0.1 copy.33
  244.6 14.4 %all-to-all-done.2 = bf16[32,36,128]{2,1,0:T(8,128)(2,1)S(1)} async-done(((bf16[32,36,128]{2,1,0:T(8,128)(2,1)}), bf16[32,36,128]{2,1,0:T(8,128)(2,1)S(1)}, u32[]{:S(2)}, u32[]{:S(2)}) %all-to-all-start.2) | async-done | bytes 294944 | tf_op jit(solution)/shard_map/all_to_all | solution.py:142
  259.0 0.1 all_to_all.26
  259.0 1.9 gather_fusion.1
  260.9 0.6 fusion.9
  261.5 0.7 add_convert_fusion
  (49 shorter events, 0.4 us)
Async XLA Ops:
  6.5 143.8 %copy-start = (bf16[1,2048,256]{2,1,0:T(8,128)(2,1)S(1)}, bf16[1,2048,256]{2,1,0:T(8,128)(2,1)}, u32[]{:S(2)}) copy-start(bf16[1,2048,256]{2,1,0:T(8,128)(2,1)} %param.23) | copy-start | bytes 3145732
  6.5 7.1 %copy-start.5 = (bf16[64,384]{1,0:T(8,128)(2,1)S(1)}, bf16[64,384]{1,0:T(8,128)(2,1)}, u32[]{:S(2)}) copy-start(bf16[64,384]{1,0:T(8,128)(2,1)} %param.14) | copy-start | bytes 147460
  6.5 7.8 %copy-start.8 = (s32[384,2]{0,1:T(2,128)S(1)}, s32[384,2]{0,1:T(2,128)}, u32[]{:S(2)}) copy-start(s32[384,2]{0,1:T(2,128)} %param.20) | copy-start | bytes 9220
  6.5 54.1 %all-gather.4.cloned.1.call-start = ((), (), s32[]{:S(2)}) async-start(), calls=%async_computation.3 | async-start | bytes 1671168 | tf_op jit(solution)/shard_map/all_gather | solution.py:25
  7.4 4.8 %collective-permute-start = (bf16[64,15]{1,0:T(8,128)(2,1)S(1)}, bf16[64,15]{1,0:T(8,128)(2,1)S(1)}, u32[]{:S(2)}, u32[]{:S(2)}) collective-permute-start(bf16[64,15]{1,0:T(8,128)(2,1)S(1)} %slice.43), channel_id=1, source_target_pairs={{0,16},{16,32},{32,48},{48,64},{64,80},{80,96},{96,112},{112,128},... | collective-permute-start | bytes 5768 | tf_op jit(solution)/shard_map/ppermute | solution.py:16
  14.4 46.3 %copy-start.2 = (bf16[4,256,256]{2,1,0:T(8,128)(2,1)S(1)}, bf16[4,256,256]{2,1,0:T(8,128)(2,1)}, u32[]{:S(2)}) copy-start(bf16[4,256,256]{2,1,0:T(8,128)(2,1)} %param.15) | copy-start | bytes 1572868
  60.6 1.6 slice-start
  60.7 2.1 copy-start.1
  60.7 2.1 copy-start.9
  62.8 1.0 copy-start.3
  62.8 1.0 copy-start.4
  62.8 13.9 %copy-start.10 = (f32[128]{0:T(128)S(1)}, f32[128]{0:T(128)}, u32[]{:S(2)}) copy-start(f32[128]{0:T(128)} %param.19) | copy-start | bytes 1540
  64.9 11.8 %all-to-all-start = ((f32[16,1,384]{2,1,0:T(1,128)}), f32[16,1,384]{2,1,0:T(1,128)S(1)}, u32[]{:S(2)}, u32[]{:S(2)}) async-start(f32[16,1,384]{2,1,0:T(1,128)} %broadcast_in_dim.69), calls=%async_computation | async-start | bytes 49152 | tf_op jit(solution)/shard_map/all_to_all | solution.py:30
  71.3 79.0 %all-gather.6.cloned.1.call-start = ((), (), s32[]{:S(2)}) async-start(), calls=%async_computation.4 | async-start | bytes 5013504 | tf_op jit(solution)/shard_map/all_gather | solution.py:130
  105.2 49.0 %copy-start.12 = (bf16[1,2048,256]{2,1,0:T(8,128)(2,1)S(1)}, bf16[1,2048,256]{2,1,0:T(8,128)(2,1)}, u32[]{:S(2)}) copy-start(bf16[1,2048,256]{2,1,0:T(8,128)(2,1)} %param.24) | copy-start | bytes 3145732
  105.2 122.9 %all-gather.8.cloned.1.call-start = ((), (), s32[]{:S(2)}) async-start(), calls=%async_computation.5 | async-start | bytes 10027008 | tf_op jit(solution)/shard_map/all_gather | solution.py:138
  150.3 3.9 %copy-start.11 = (bf16[1152,2048]{1,0:T(8,128)(2,1)S(1)}, bf16[1152,2048]{1,0:T(8,128)(2,1)}, u32[]{:S(2)}) copy-start(bf16[1152,2048]{1,0:T(8,128)(2,1)} %all-gather.6.cloned.1.call-done) | copy-start | bytes 14155780
  154.2 2.4 copy-start.6
  156.7 87.7 %copy-start.7 = (f32[384,2]{0,1:T(2,128)S(1)}, f32[384,2]{0,1:T(2,128)}, u32[]{:S(2)}) copy-start(f32[384,2]{0,1:T(2,128)} %param.22) | copy-start | bytes 9220
  235.3 23.6 %all-to-all-start.2 = ((bf16[32,36,128]{2,1,0:T(8,128)(2,1)}), bf16[32,36,128]{2,1,0:T(8,128)(2,1)S(1)}, u32[]{:S(2)}, u32[]{:S(2)}) async-start(bf16[32,36,128]{2,1,0:T(8,128)(2,1)} %all_to_all.24), calls=%async_computation.2 | async-start | bytes 655360 | tf_op jit(solution)/shard_map/all_to_all | solution.py:142
Sparse Core Ops, SparseCore 0:
  14.5 46.1 all-gather.3
  105.3 44.9 all-gather.5
  156.7 71.2 all-gather.7
where the time goes:
time: 269 us
  waiting for transfers between devices  178 us (66%)
  blocking collectives  24.5 us (9%)
  starting transfers between devices  18.8 us (7%)
  local copies, waits for them, and re-layouts  14.7 us (5%)
  matrix products  13.7 us (5%)
  between operations  13.5 us (5%)
  other arithmetic  5.95 us (2%)
    all_gather x1, waiting for transfers between devices, per_device(): lax.all_gather(activated, 'tp', axis=1, tiled=True)  71.4 us
    all_gather x1, waiting for transfers between devices, per_device(): portion = lax.all_gather(arrived, 'tp', axis=1, tiled=True)  45.1 us
    all_gather x1, waiting for transfers between devices, in_one_piece(): lax.all_gather(both, axis, axis=dim, tiled=True)  39.9 us
    all_to_all x1, blocking collectives, per_device(): lax.all_to_all(padded[sources], 'sp', split_axis=0, concat_axis=0, tiled=...  24.5 us
    all_to_all x1, waiting for transfers between devices, per_device(): lax.all_to_all(result, 'sp', split_axis=0, concat_axis=0, tiled=True)  14.4 us
    all_to_all x1, starting transfers between devices, per_device(): lax.all_to_all(result, 'sp', split_axis=0, concat_axis=0, tiled=True)  8.98 us
    dot_general x1, matrix products, per_device(): jnp.dot(lax.all_gather(activated, 'tp', axis=1, tiled=True), rows_down, p...  6.52 us
    all_to_all x1, starting transfers between devices, from_everyone(): lax.all_to_all(jnp.broadcast_to(value[None], (count, *value.shape)), axis...  6.36 us
  transfers between devices with their start and end apart: 6, of which 6 were waited for; matrix products, arithmetic and copies ran while one was open for 2% of the time, Pallas kernels for 0%

commit v1 on v0

--- a/solution.py
+++ b/solution.py
@@ -8,6 +8,14 @@
 TOP = 2
 reach_back = 15
 epsilon = 1e-06
+
+
+def tiled_gather(shard, axis, dim):
+    devices = lax.axis_size(axis)
+    repeats = [devices if d == dim else 1 for d in range(shard.ndim)]
+    return lax.all_to_all(
+        jnp.tile(shard, repeats), axis, split_axis=dim, concat_axis=dim, tiled=True
+    )
 
 
 def from_behind(value, axis, steps):
@@ -135,9 +143,7 @@
     activated = (jax.nn.silu(gate_term) * up_term).astype(jnp.bfloat16)
     rows_down = w_down[0]
     result = jnp.dot(
-        lax.all_gather(activated, "tp", axis=1, tiled=True),
-        rows_down,
-        preferred_element_type=jnp.float32,
+        tiled_gather(activated, "tp", 1), rows_down, preferred_element_type=jnp.float32
     ).astype(jnp.bfloat16)
     returned = lax.all_to_all(result, "sp", split_axis=0, concat_axis=0, tiled=True)
     picked = returned[destination].astype(jnp.float32).reshape(length, TOP, returned.shape[1])

time: 269 us -> 428 us (1.59)
  the two profiles are of different devices: /device:TPU:16 before, /device:TPU:24 now
where the time goes in v1:
time: 428 us; the launch traced here: 427 us
  waiting for transfers between devices  313 us (73%)
  local copies, waits for them, and re-layouts  32 us (7%)
  starting transfers between devices  25 us (6%)
  blocking collectives  24.5 us (6%)
  between operations  13.8 us (3%)
  matrix products  12.8 us (3%)
  other arithmetic  5.95 us (1%)
    all_to_all x1, waiting for transfers between devices, tiled_gather(): lax.all_to_all(jnp.tile(shard, repeats), axis, split_axis=dim, concat_axi...  206 us
    all_gather x1, waiting for transfers between devices, per_device(): portion = lax.all_gather(arrived, 'tp', axis=1, tiled=True)  45.8 us
    all_gather x1, waiting for transfers between devices, in_one_piece(): lax.all_gather(both, axis, axis=dim, tiled=True)  41 us
    all_to_all x1, blocking collectives, per_device(): lax.all_to_all(padded[sources], 'sp', split_axis=0, concat_axis=0, tiled=...  24.5 us
    all_to_all x1, waiting for transfers between devices, per_device(): lax.all_to_all(result, 'sp', split_axis=0, concat_axis=0, tiled=True)  14.2 us
    all_to_all x1, local copies, waits for them, and re-layouts, tiled_gather(): lax.all_to_all(jnp.tile(shard, repeats), axis, split_axis=dim, concat_axi...  12.8 us
    all_to_all x1, starting transfers between devices, per_device(): lax.all_to_all(result, 'sp', split_axis=0, concat_axis=0, tiled=True)  9.07 us
  transfers between devices with their start and end apart: 6, of which 6 were waited for; matrix products, arithmetic and copies ran while one was open for 2% of the time, Pallas kernels for 0%

profile of v1, /device:TPU:24, one launch (start us, length us, event | category | flops | bytes accessed | tf_op | source)
XLA Modules:
  0.0 427.0 jit_solution(15807973357118824054)
XLA Ops:
  6.5 0.9 slice.43
  7.4 3.4 collective-permute-start
  10.9 1.3 collective-permute-done
  12.2 0.9 maximum_convert_fusion
  13.1 0.1 slice_add_fusion.2
  13.2 0.1 slice_add_fusion.1
  13.3 0.1 slice_add_fusion
  13.5 0.2 fusion.13
  13.7 0.7 pad_maximum_fusion
  14.4 0.1 copy.54
  14.5 0.1 eq.69
  14.7 0.1 eq.65
  14.8 1.7 reduce-window.6
  16.6 0.3 slice_reduce_fusion
  16.9 0.1 copy.53
  17.0 0.2 mul.134
  17.2 0.1 fusion.12
  17.3 3.4 scatter_custom_fusion
  20.7 41.0 %all-gather.3.cloned.1.call-done = bf16[1024,768]{1,0:T(8,128)(2,1)} async-done(((bf16[64,768]{1,0:T(8,128)(2,1)}), bf16[1024,768]{1,0:T(8,128)(2,1)}) %all-gather.3.cloned.1.call-update) | async-done | bytes 1572880 | tf_op jit(solution)/shard_map/all_gather | solution.py:33
  61.8 1.6 slice-done
  63.4 0.5 fusion.26
  64.0 0.4 fusion.2
  64.4 0.5 copy-done.3
  64.9 0.5 multiply_reduce_fusion
  65.4 0.6 broadcast_in_dim.69
  66.0 5.1 %all-to-all-start = ((f32[16,1,384]{2,1,0:T(1,128)}), f32[16,1,384]{2,1,0:T(1,128)S(1)}, u32[]{:S(2)}, u32[]{:S(2)}) async-start(f32[16,1,384]{2,1,0:T(1,128)} %broadcast_in_dim.69), calls=%async_computation | async-start | bytes 49152 | tf_op jit(solution)/shard_map/all_to_all | solution.py:38
  71.2 4.5 %all-to-all-done = f32[16,1,384]{2,1,0:T(1,128)S(1)} async-done(((f32[16,1,384]{2,1,0:T(1,128)}), f32[16,1,384]{2,1,0:T(1,128)S(1)}, u32[]{:S(2)}, u32[]{:S(2)}) %all-to-all-start) | async-done | bytes 24608 | tf_op jit(solution)/shard_map/all_to_all | solution.py:38
  75.8 0.1 multiply_convert_fusion
  75.9 2.9 gather_fusion
  78.8 0.1 all_to_all.27
  78.9 24.5 %all_to_all.39 = bf16[32,36,128]{2,1,0:T(8,128)(2,1)S(1)} all-to-all(bf16[32,36,128]{2,1,0:T(8,128)(2,1)S(1)} %all_to_all.27), channel_id=1, replica_groups=mesh['sp'=32,'tp'=16] {'sp'}, dimensions={0} | all-to-all | bytes 589824 | tf_op jit(solution)/shard_map/all_to_all | solution.py:137
  103.4 0.8 all_to_all.29
  104.2 45.8 %all-gather.5.cloned.1.call-done = bf16[1152,2048]{1,0:T(8,128)(2,1)} async-done(((bf16[1152,128]{1,0:T(8,128)(2,1)}), bf16[1152,2048]{1,0:T(8,128)(2,1)}) %all-gather.5.cloned.1.call-update) | async-done | bytes 4718608 | tf_op jit(solution)/shard_map/all_gather | solution.py:138
  150.0 3.9 fusion.7
  153.9 1.6 fusion
  155.5 4.6 %tile.2 = bf16[1152,16,256]{2,0,1:T(8,128)(2,1)} broadcast(bf16[1152,256]{1,0:T(8,128)(2,1)S(1)} %fusion), dimensions={0,2} | broadcast | bytes 10027008 | tf_op jit(solution)/shard_map/tile | solution.py:17
  160.1 7.4 %all-to-all-start.2 = ((bf16[1152,16,256]{2,0,1:T(8,128)(2,1)}), bf16[1152,16,256]{2,0,1:T(8,128)(2,1)}, u32[]{:S(2)}, u32[]{:S(2)}) async-start(bf16[1152,16,256]{2,0,1:T(8,128)(2,1)} %tile.2), calls=%async_computation.2 | async-start | bytes 18874368 | tf_op jit(solution)/shard_map/all_to_all | solution.py:16
  167.5 206.0 %all-to-all-done.2 = bf16[1152,16,256]{2,0,1:T(8,128)(2,1)} async-done(((bf16[1152,16,256]{2,0,1:T(8,128)(2,1)}), bf16[1152,16,256]{2,0,1:T(8,128)(2,1)}, u32[]{:S(2)}, u32[]{:S(2)}) %all-to-all-start.2) | async-done | bytes 9437216 | tf_op jit(solution)/shard_map/all_to_all | solution.py:16
  373.5 12.8 %copy.57 = bf16[1152,16,256]{0,2,1:T(8,128)(2,1)} copy(bf16[1152,16,256]{2,0,1:T(8,128)(2,1)} %all-to-all-done.2) | data formatting | bytes 18874368 | tf_op jit(solution)/shard_map/all_to_all | solution.py:16
  386.3 6.4 %convolution_convert_fusion = bf16[1152,128]{1,0:T(8,128)(2,1)S(1)} fusion(bf16[1152,4096]{0,1:T(8,128)(2,1)} %bitcast.50, bf16[1,4096,128]{2,1,0:T(8,128)(2,1)S(1)} %copy-done.13), kind=kOutput, calls=%fused_computation.5 | convolution fusion | flops 1208107008 | bytes 10780672 | tf_op jit(solution)/shard_map/dot_general | solution.py:145
  392.6 0.8 all_to_all.32
  393.4 9.1 %all-to-all-start.3 = ((bf16[32,36,128]{2,1,0:T(8,128)(2,1)}), bf16[32,36,128]{2,1,0:T(8,128)(2,1)S(1)}, u32[]{:S(2)}, u32[]{:S(2)}) async-start(bf16[32,36,128]{2,1,0:T(8,128)(2,1)} %all_to_all.32), calls=%async_computation.3 | async-start | bytes 655360 | tf_op jit(solution)/shard_map/all_to_all | solution.py:148
  402.6 0.1 copy.51
  402.7 14.2 %all-to-all-done.3 = bf16[32,36,128]{2,1,0:T(8,128)(2,1)S(1)} async-done(((bf16[32,36,128]{2,1,0:T(8,128)(2,1)}), bf16[32,36,128]{2,1,0:T(8,128)(2,1)S(1)}, u32[]{:S(2)}, u32[]{:S(2)}) %all-to-all-start.3) | async-done | bytes 294944 | tf_op jit(solution)/shard_map/all_to_all | solution.py:148
  417.0 0.1 all_to_all.34
  417.1 1.9 gather_fusion.1
  418.9 0.6 fusion.9
  419.5 0.7 add_convert_fusion
  (52 shorter events, 0.4 us)
Async XLA Ops:
  6.5 143.5 %copy-start = (bf16[1,2048,256]{2,1,0:T(8,128)(2,1)S(1)}, bf16[1,2048,256]{2,1,0:T(8,128)(2,1)}, u32[]{:S(2)}) copy-start(bf16[1,2048,256]{2,1,0:T(8,128)(2,1)} %param.23) | copy-start | bytes 3145732
  6.5 7.1 %copy-start.5 = (bf16[64,384]{1,0:T(8,128)(2,1)S(1)}, bf16[64,384]{1,0:T(8,128)(2,1)}, u32[]{:S(2)}) copy-start(bf16[64,384]{1,0:T(8,128)(2,1)} %param.14) | copy-start | bytes 147460
  6.5 7.8 %copy-start.8 = (s32[384,2]{0,1:T(2,128)S(1)}, s32[384,2]{0,1:T(2,128)}, u32[]{:S(2)}) copy-start(s32[384,2]{0,1:T(2,128)} %param.20) | copy-start | bytes 9220
  6.5 55.2 %all-gather.3.cloned.1.call-start = ((), (), s32[]{:S(2)}) async-start(), calls=%async_computation.4 | async-start | bytes 1671168 | tf_op jit(solution)/shard_map/all_gather | solution.py:33
  7.4 4.8 %collective-permute-start = (bf16[64,15]{1,0:T(8,128)(2,1)S(1)}, bf16[64,15]{1,0:T(8,128)(2,1)S(1)}, u32[]{:S(2)}, u32[]{:S(2)}) collective-permute-start(bf16[64,15]{1,0:T(8,128)(2,1)S(1)} %slice.43), channel_id=1, source_target_pairs={{0,16},{16,32},{32,48},{48,64},{64,80},{80,96},{96,112},{112,128},... | collective-permute-start | bytes 5768 | tf_op jit(solution)/shard_map/ppermute | solution.py:24
  14.4 47.4 %copy-start.2 = (bf16[4,256,256]{2,1,0:T(8,128)(2,1)S(1)}, bf16[4,256,256]{2,1,0:T(8,128)(2,1)}, u32[]{:S(2)}) copy-start(bf16[4,256,256]{2,1,0:T(8,128)(2,1)} %param.15) | copy-start | bytes 1572868
  61.8 1.6 slice-start
  61.8 2.1 copy-start.1
  61.8 2.1 copy-start.9
  63.9 1.0 copy-start.3
  63.9 1.0 copy-start.4
  64.0 11.8 %copy-start.10 = (f32[128]{0:T(128)S(1)}, f32[128]{0:T(128)}, u32[]{:S(2)}) copy-start(f32[128]{0:T(128)} %param.19) | copy-start | bytes 1540
  66.0 9.7 %all-to-all-start = ((f32[16,1,384]{2,1,0:T(1,128)}), f32[16,1,384]{2,1,0:T(1,128)S(1)}, u32[]{:S(2)}, u32[]{:S(2)}) async-start(f32[16,1,384]{2,1,0:T(1,128)} %broadcast_in_dim.69), calls=%async_computation | async-start | bytes 49152 | tf_op jit(solution)/shard_map/all_to_all | solution.py:38
  71.1 78.9 %all-gather.5.cloned.1.call-start = ((), (), s32[]{:S(2)}) async-start(), calls=%async_computation.5 | async-start | bytes 5013504 | tf_op jit(solution)/shard_map/all_gather | solution.py:138
  104.2 49.7 %copy-start.12 = (bf16[1,2048,256]{2,1,0:T(8,128)(2,1)S(1)}, bf16[1,2048,256]{2,1,0:T(8,128)(2,1)}, u32[]{:S(2)}) copy-start(bf16[1,2048,256]{2,1,0:T(8,128)(2,1)} %param.24) | copy-start | bytes 3145732
  150.0 3.9 copy-start.11
  160.1 7.4 %copy-start.6 = (f32[384,4]{0,1:T(4,128)S(1)}, f32[384,4]{0,1:T(4,128)}, u32[]{:S(2)}) copy-start(f32[384,4]{0,1:T(4,128)} %param.21) | copy-start | bytes 18436
  160.1 213.4 %all-to-all-start.2 = ((bf16[1152,16,256]{2,0,1:T(8,128)(2,1)}), bf16[1152,16,256]{2,0,1:T(8,128)(2,1)}, u32[]{:S(2)}, u32[]{:S(2)}) async-start(bf16[1152,16,256]{2,0,1:T(8,128)(2,1)} %tile.2), calls=%async_computation.2 | async-start | bytes 18874368 | tf_op jit(solution)/shard_map/all_to_all | solution.py:16
  167.5 218.8 %copy-start.13 = (bf16[1,4096,128]{2,1,0:T(8,128)(2,1)S(1)}, bf16[1,4096,128]{2,1,0:T(8,128)(2,1)}, u32[]{:S(2)}) copy-start(bf16[1,4096,128]{2,1,0:T(8,128)(2,1)} %param.25) | copy-start | bytes 3145732
  386.3 16.2 %copy-start.7 = (f32[384,2]{0,1:T(2,128)S(1)}, f32[384,2]{0,1:T(2,128)}, u32[]{:S(2)}) copy-start(f32[384,2]{0,1:T(2,128)} %param.22) | copy-start | bytes 9220
  393.4 23.6 %all-to-all-start.3 = ((bf16[32,36,128]{2,1,0:T(8,128)(2,1)}), bf16[32,36,128]{2,1,0:T(8,128)(2,1)S(1)}, u32[]{:S(2)}, u32[]{:S(2)}) async-start(bf16[32,36,128]{2,1,0:T(8,128)(2,1)} %all_to_all.32), calls=%async_computation.3 | async-start | bytes 655360 | tf_op jit(solution)/shard_map/all_to_all | solution.py:148
Sparse Core Ops, SparseCore 0:
  14.5 47.2 all-gather.2
  104.3 45.6 all-gather.4
